TPU v7x, 32 devices: a whole 2x2x4 slice. The times are simulated.
32 devices in a mesh: grp: 2 (over y), fs: 4 (over z), tp: 4 (over x, core).
Axes of the slice: x: 2, y: 2, z: 4, core: 2. Of those that a mesh axis runs over, the one named last changes fastest.
Arguments:
- tokens: bfloat16 [8, 384, 2048], P(('grp', 'fs'), None, 'tp'), parts along dimension 0, may hold values from -16 to 16
- norm_gain: float32 [2048], P('tp'), may hold values from 0.1 to 1.9
- in_weight: bfloat16 [2048, 1024], P('fs', 'tp'), may hold values from -0.125 to 0.125
- pool_weight: bfloat16 [8, 128, 128], P('tp'), may hold values from -0.5 to 0.5
- pool_scale: float32 [1024], P('tp'), may hold values from 0.1 to 1.9
- out_weight: bfloat16 [1024, 2048], P('fs', 'tp'), may hold values from -0.1875 to 0.1875
- ffn_gain: float32 [2048], P('tp'), may hold values from 0.1 to 1.9
- gate_weight: bfloat16 [2048, 5632], P('fs', 'tp'), may hold values from -0.125 to 0.125
- up_weight: bfloat16 [2048, 5632], P('fs', 'tp'), may hold values from -0.125 to 0.125
- down_weight: bfloat16 [5632, 2048], P('tp', 'fs'), may hold values from -0.078125 to 0.078125
Outputs:
- output: bfloat16 [8, 384, 2048], P(('grp', 'fs'), None, 'tp'), parts along dimension 0
There are 2 independent parts, one for each index of `grp`. A program takes and returns all parts, laid end to end along the dimension named above; an argument that names none is the same for every part. Nothing has to cross between parts.
All inputs are finite; a program needn't handle non-finite values.
Results may differ from a plain program's by a relative error of at most 0.009.
Values may be sent and summed in bfloat16 or wider, within the bound.
A program may use at most 64 MiB of HBM per device.

v0:
```python
import jax
import jax.numpy as jnp
from jax import lax
from jax.sharding import PartitionSpec as P

D = 2048
GD = 128
EPSILON = 0.05
HALVES = (1, 2, 4, 8)


def local(
    tokens,
    norm_gain,
    in_weight,
    pool_weight,
    pool_scale,
    out_weight,
    ffn_gain,
    gate_weight,
    up_weight,
    down_weight,
):
    seq_local, length, feat_local = tokens.shape
    stream = tokens.astype(jnp.float32)
    first_square = lax.psum(jnp.sum(stream * stream, axis=-1), "tp")
    normed = (stream * lax.rsqrt(first_square[..., None] / D + EPSILON) * norm_gain).astype(
        jnp.bfloat16
    )
    in_full = lax.all_gather(in_weight, "fs", axis=0, tiled=True)
    channels = in_full.shape[1]
    weight_rows = in_full
    pool_input = jnp.einsum(
        "slk,kc->slc",
        lax.all_gather(normed, "tp", axis=2, tiled=True),
        weight_rows,
        preferred_element_type=jnp.float32,
    ).astype(jnp.bfloat16)
    pool_float = pool_input.astype(jnp.float32)
    group_local = pool_weight.shape[0]
    group_ids = lax.axis_index("tp") * group_local + jnp.arange(channels) // GD
    selector = group_ids % 4
    running = jnp.concatenate(
        [jnp.zeros((seq_local, 1, channels), jnp.float32), jnp.cumsum(pool_float, axis=1)], axis=1
    )
    position = jnp.arange(length)
    window_mean = jnp.zeros_like(pool_float)
    for window_index, half_width in enumerate(HALVES):
        upper_sum = jnp.concatenate(
            [running[:, half_width:], jnp.repeat(running[:, -1:], half_width, axis=1)], axis=1
        )[:, :length]
        lower_sum = jnp.concatenate(
            [
                jnp.zeros((seq_local, half_width, channels), jnp.float32),
                running[:, : length + 1 - half_width],
            ],
            axis=1,
        )[:, :length]
        counts = (
            jnp.minimum(position + half_width, length) - jnp.maximum(position - half_width, 0)
        ).astype(jnp.float32)
        window_mean = jnp.where(
            selector == window_index, (upper_sum - lower_sum) / counts[:, None], window_mean
        )
    deviation = (window_mean - pool_float).astype(jnp.bfloat16)
    grouped = deviation.reshape(seq_local, length, group_local, GD)
    mapped = jnp.einsum("slgc,gcd->slgd", grouped, pool_weight, preferred_element_type=jnp.float32)
    pooled = (mapped.reshape(seq_local, length, channels) * pool_scale).astype(jnp.bfloat16)
    out_full = lax.all_gather(out_weight, "fs", axis=0, tiled=True)
    weight_rows = out_full
    mixed = stream + jnp.einsum(
        "jut,tx->jux",
        lax.all_gather(pooled, "tp", axis=2, tiled=True),
        weight_rows,
        preferred_element_type=jnp.float32,
    )
    second_square = lax.psum(jnp.sum(mixed * mixed, axis=-1), "tp")
    normed_two = (mixed * lax.rsqrt(second_square[..., None] / D + EPSILON) * ffn_gain).astype(
        jnp.bfloat16
    )
    features_full = lax.all_gather(normed_two, "tp", axis=2, tiled=True)
    gate_sum = jnp.einsum(
        "slk,kf->slf",
        features_full,
        lax.all_gather(gate_weight, "fs", axis=0, tiled=True),
        preferred_element_type=jnp.float32,
    )
    up_sum = jnp.einsum(
        "slk,kf->slf",
        features_full,
        lax.all_gather(up_weight, "fs", axis=0, tiled=True),
        preferred_element_type=jnp.float32,
    )
    hidden = (jax.nn.silu(gate_sum) * up_sum).astype(jnp.bfloat16)
    partial_value = jnp.einsum(
        "hor,rn->hon",
        hidden,
        lax.all_gather(down_weight, "fs", axis=1, tiled=True),
        preferred_element_type=jnp.float32,
    )
    summed = lax.psum_scatter(
        partial_value.astype(jnp.bfloat16), "tp", scatter_dimension=2, tiled=True
    ).astype(jnp.float32)
    return (mixed + summed).astype(jnp.bfloat16)


def solution(mesh):
    return jax.shard_map(
        local,
        mesh=mesh,
        in_specs=(
            P(("grp", "fs"), None, "tp"),
            P("tp"),
            P("fs", "tp"),
            P("tp", None, None),
            P("tp"),
            P("fs", "tp"),
            P("tp"),
            P("fs", "tp"),
            P("fs", "tp"),
            P("tp", "fs"),
        ),
        out_specs=P(("grp", "fs"), None, "tp"),
        check_vma=False,
    )
```

profile of v0, /device:TPU:0, one launch (start us, length us, event | category | flops | bytes accessed | tf_op | source)
XLA Modules:
  0.0 485.2 jit_solution(12671679941246397171)
XLA Ops:
  6.5 0.7 all-gather.10.cloned.1.call-update
  7.3 1.2 fusion.17
  8.5 8.4 %psum.14 = f32[1,384]{1,0:T(1,128)S(1)} all-reduce(f32[1,384]{1,0:T(1,128)S(1)} %reduce_sum.23), channel_id=1, replica_groups=mesh['grp'=2,'fs'=4,'tp'=4] {'tp'}, use_global_device_ids=true, to_apply=%region_1.0 | all-reduce | flops 384 | bytes 3072 | tf_op jit(solution)/shard_map/psum | solution.py:26
  16.9 1.9 fusion.19
  18.8 0.7 all-gather.12.cloned.1.call-update
  19.6 20.0 %all-gather.10.cloned.1.call-done = bf16[2048,256]{1,0:T(8,128)(2,1)} async-done(((bf16[512,256]{1,0:T(8,128)(2,1)}), bf16[2048,256]{1,0:T(8,128)(2,1)}) %all-gather.10.cloned.1.call-update) | async-done | bytes 1048592 | tf_op jit(solution)/shard_map/all_gather | solution.py:30
  39.6 20.6 %all-gather.8.cloned.1.call-done = bf16[1,384,2048]{2,1,0:T(8,128)(2,1)} async-done(((bf16[1,384,512]{2,1,0:T(8,128)(2,1)}), bf16[1,384,2048]{2,1,0:T(8,128)(2,1)}) %all-gather.8.cloned.1.call-update) | async-done | bytes 1572880 | tf_op jit(solution)/shard_map/all_gather | solution.py:35
  60.2 2.3 fusion.14
  62.5 0.3 fusion.23
  62.8 0.1 copy.12
  63.0 0.1 fusion.63
  63.1 0.1 fusion.61
  63.1 0.1 fusion.62
  63.3 0.5 fusion.39
  63.8 0.3 fusion.40
  64.1 0.1 fusion.38
  64.2 8.6 %all_gather.26 = bf16[1,384,1024]{1,2,0:T(8,128)(2,1)S(1)} all-gather(bf16[1,384,256]{1,2,0:T(8,128)(2,1)S(1)} %fusion.38), channel_id=1, replica_groups=mesh['grp'=2,'fs'=4,'tp'=4] {'tp'}, dimensions={2}, use_global_device_ids=true | all-gather | bytes 983040 | tf_op jit(solution)/shard_map/all_gather | solution.py:73
  72.8 17.0 %all-gather.12.cloned.1.call-done = bf16[1024,512]{1,0:T(8,128)(2,1)} async-done(((bf16[256,512]{1,0:T(8,128)(2,1)}), bf16[1024,512]{1,0:T(8,128)(2,1)}) %all-gather.12.cloned.1.call-update) | async-done | bytes 1048592 | tf_op jit(solution)/shard_map/all_gather | solution.py:69
  89.8 1.9 multiply_reduce_fusion
  91.8 6.1 %psum.15 = f32[1,384]{1,0:T(1,128)S(1)} all-reduce(f32[1,384]{1,0:T(1,128)S(1)} %reduce_sum.25), channel_id=1, replica_groups=mesh['grp'=2,'fs'=4,'tp'=4] {'tp'}, use_global_device_ids=true, to_apply=%region_5.6 | all-reduce | flops 384 | bytes 3072 | tf_op jit(solution)/shard_map/psum | solution.py:77
  97.9 0.9 multiply_convert_fusion
  98.8 0.5 all-gather.16.cloned.1.call-update
  99.4 0.5 all-gather.18.cloned.1.call-update
  100.0 0.7 all-gather.20.cloned.1.call-update
  100.7 17.0 %all-gather.14.cloned.1.call-done = bf16[1,384,2048]{2,1,0:T(8,128)(2,1)} async-done(((bf16[1,384,512]{2,1,0:T(8,128)(2,1)}), bf16[1,384,2048]{2,1,0:T(8,128)(2,1)}) %all-gather.14.cloned.1.call-update) | async-done | bytes 1572880 | tf_op jit(solution)/shard_map/all_gather | solution.py:81
  117.8 108.1 %all-gather.16.cloned.1.call-done = bf16[2048,1408]{1,0:T(8,128)(2,1)} async-done(((bf16[512,1408]{1,0:T(8,128)(2,1)}), bf16[2048,1408]{1,0:T(8,128)(2,1)}) %all-gather.16.cloned.1.call-update) | async-done | bytes 5767184 | tf_op jit(solution)/shard_map/all_gather | solution.py:85
  225.9 7.1 %fusion.3 = f32[384,1408]{1,0:T(8,128)} fusion(bf16[2048,1408]{1,0:T(8,128)(2,1)} %all-gather.16.cloned.1.call-done, bf16[1,384,2048]{2,1,0:T(8,128)(2,1)} %all-gather.14.cloned.1.call-done), kind=kOutput, calls=%fused_computation.5 | convolution fusion | flops 2214592512 | bytes 9502720 | tf_op jit(solution)/shard_map/slk,kf->slf/dot_general | solution.py:82
  233.0 99.3 %all-gather.18.cloned.1.call-done = bf16[2048,1408]{1,0:T(8,128)(2,1)} async-done(((bf16[512,1408]{1,0:T(8,128)(2,1)}), bf16[2048,1408]{1,0:T(8,128)(2,1)}) %all-gather.18.cloned.1.call-update) | async-done | bytes 5767184 | tf_op jit(solution)/shard_map/all_gather | solution.py:91
  332.3 106.5 %all-gather.20.cloned.1.call-done = bf16[1408,2048]{1,0:T(8,128)(2,1)} async-done(((bf16[1408,512]{1,0:T(8,128)(2,1)}), bf16[1408,2048]{1,0:T(8,128)(2,1)}) %all-gather.20.cloned.1.call-update) | async-done | bytes 5767184 | tf_op jit(solution)/shard_map/all_gather | solution.py:98
  438.9 11.3 %fusion.1 = bf16[1,384,2048]{2,1,0:T(8,128)(2,1)} fusion(bf16[1408,2048]{1,0:T(8,128)(2,1)} %all-gather.20.cloned.1.call-done, bf16[2048,1408]{1,0:T(8,128)(2,1)} %all-gather.18.cloned.1.call-done, f32[384,1408]{1,0:T(8,128)} %fusion.3, bf16[1,384,2048]{2,1,0:T(8,128)(2,1)S(1)} %copy-done.4), kind=kOutput, calls=%fused_computation.3 | convolution fusion | flops 4433215488 | bytes 16842752 | tf_op jit(solution)/shard_map/hor,rn->hon/dot_general | solution.py:95
  450.2 26.4 %reduce-scatter.2.cloned.1.call-done = bf16[1,384,512]{2,1,0:T(8,128)(2,1)} async-done(((bf16[1,384,2048]{2,1,0:T(8,128)(2,1)}), bf16[1,384,512]{2,1,0:T(8,128)(2,1)}) %reduce-scatter.2.cloned.1.call-update) | async-done | bytes 393232 | tf_op jit(solution)/shard_map/reduce_scatter | solution.py:101
  476.5 1.9 add_convert_fusion
  (39 shorter events, 0.6 us)
Async XLA Ops:
  6.5 57.3 %copy-start = (bf16[2,128,128]{2,1,0:T(8,128)(2,1)S(1)}, bf16[2,128,128]{2,1,0:T(8,128)(2,1)}, u32[]{:S(2)}) copy-start(bf16[2,128,128]{2,1,0:T(8,128)(2,1)} %param.13) | copy-start | bytes 196612
  6.5 33.1 %all-gather.10.cloned.1.call-start = ((), (), s32[]{:S(2)}) async-start(), calls=%async_computation.2 | async-start | bytes 1310720 | tf_op jit(solution)/shard_map/all_gather | solution.py:30
  7.3 53.0 %all-gather.8.cloned.1.call-start = ((), (), s32[]{:S(2)}) async-start(), calls=%async_computation.1 | async-start | bytes 1966080 | tf_op jit(solution)/shard_map/all_gather | solution.py:35
  18.8 71.0 %all-gather.12.cloned.1.call-start = ((), (), s32[]{:S(2)}) async-start(), calls=%async_computation.3 | async-start | bytes 1310720 | tf_op jit(solution)/shard_map/all_gather | solution.py:69
  19.5 98.3 %all-gather.14.cloned.1.call-start = ((), (), s32[]{:S(2)}) async-start(), calls=%async_computation.4 | async-start | bytes 1966080 | tf_op jit(solution)/shard_map/all_gather | solution.py:81
  63.2 0.9 copy-start.3
  63.8 26.1 %copy-start.1 = (bf16[1,384,512]{2,1,0:T(8,128)(2,1)S(1)}, bf16[1,384,512]{2,1,0:T(8,128)(2,1)}, u32[]{:S(2)}) copy-start(bf16[1,384,512]{2,1,0:T(8,128)(2,1)} %param.10) | copy-start | bytes 1179652
  64.2 33.6 %copy-start.2 = (f32[512]{0:T(512)S(1)}, f32[512]{0:T(512)}, u32[]{:S(2)}) copy-start(f32[512]{0:T(512)} %param.16) | copy-start | bytes 6148
  98.8 127.2 %all-gather.16.cloned.1.call-start = ((), (), s32[]{:S(2)}) async-start(), calls=%async_computation.5 | async-start | bytes 7208960 | tf_op jit(solution)/shard_map/all_gather | solution.py:85
  99.4 233.0 %all-gather.18.cloned.1.call-start = ((), (), s32[]{:S(2)}) async-start(), calls=%async_computation.6 | async-start | bytes 7208960 | tf_op jit(solution)/shard_map/all_gather | solution.py:91
  99.9 338.9 %all-gather.20.cloned.1.call-start = ((), (), s32[]{:S(2)}) async-start(), calls=%async_computation.7 | async-start | bytes 7208960 | tf_op jit(solution)/shard_map/all_gather | solution.py:98
  100.7 375.8 %reduce-scatter.2.cloned.1.call-start = ((), (), s32[]{:S(2)}) async-start(), calls=%async_computation.8 | async-start | bytes 1966080 | tf_op jit(solution)/shard_map/reduce_scatter | solution.py:101
  117.8 321.1 %copy-start.4 = (bf16[1,384,2048]{2,1,0:T(8,128)(2,1)S(1)}, bf16[1,384,2048]{2,1,0:T(8,128)(2,1)}, u32[]{:S(2)}) copy-start(bf16[1,384,2048]{2,1,0:T(8,128)(2,1)} %all-gather.14.cloned.1.call-done) | copy-start | bytes 4718596
Sparse Core Ops, SparseCore 0:
  8.9 30.6 all-gather.9
  41.2 18.9 all-gather.7
  61.8 27.9 all-gather.11
  98.9 18.8 all-gather.13
  119.2 106.6 all-gather.15
  227.4 104.9 all-gather.17
  333.9 104.9 all-gather.19
  450.3 26.2 reduce-scatter.1
where the time goes:
time: 486 us; the launch traced here: 485 us
  waiting for transfers between devices  418 us (86%)
  blocking collectives  23 us (5%)
  matrix products  22.8 us (5%)
  between operations  13.7 us (3%)
  other arithmetic  6.86 us (1%)
    all_gather x1, waiting for transfers between devices, local(): lax.all_gather(gate_weight, 'fs', axis=0, tiled=True)  108 us
    all_gather x1, waiting for transfers between devices, local(): lax.all_gather(down_weight, 'fs', axis=1, tiled=True)  107 us
    all_gather x1, waiting for transfers between devices, local(): lax.all_gather(up_weight, 'fs', axis=0, tiled=True)  99.3 us
    reduce_scatter x1, waiting for transfers between devices, local(): lax.psum_scatter(partial_value.astype(jnp.bfloat16), 'tp', scatter_dimens...  26.4 us
    all_gather x1, waiting for transfers between devices, local(): lax.all_gather(normed, 'tp', axis=2, tiled=True)  20.6 us
    all_gather x1, waiting for transfers between devices, local(): in_full = lax.all_gather(in_weight, 'fs', axis=0, tiled=True)  20 us
    all_gather x1, waiting for transfers between devices, local(): features_full = lax.all_gather(normed_two, 'tp', axis=2, tiled=True)  17 us
    all_gather x1, waiting for transfers between devices, local(): out_full = lax.all_gather(out_weight, 'fs', axis=0, tiled=True)  17 us
  transfers between devices with their start and end apart: 8, of which 8 were waited for; matrix products, arithmetic and copies ran while one was open for 3% of the time, Pallas kernels for 0%

commit v1 on v0

--- a/solution.py
+++ b/solution.py
@@ -7,6 +7,21 @@
 GD = 128
 EPSILON = 0.05
 HALVES = (1, 2, 4, 8)
+
+
+def on_each_block(x, axis, dim, make, out_dim):
+    ways, here, step = (lax.axis_size(axis), lax.axis_index(axis), x.shape[dim])
+    results = []
+    for far in range(ways):
+        arriving = (
+            lax.ppermute(x, axis, [(d, (d + 1) % ways) for d in range(ways)])
+            if far + 1 < ways
+            else x
+        )
+        results.append(make(x, (here - far) % ways * step))
+        x = arriving
+    line = jnp.concatenate(results[::-1], axis=out_dim)
+    return jnp.roll(line, (here + 1) * results[0].shape[out_dim], axis=out_dim)
 
 
 def local(
@@ -92,11 +107,14 @@
         preferred_element_type=jnp.float32,
     )
     hidden = (jax.nn.silu(gate_sum) * up_sum).astype(jnp.bfloat16)
-    partial_value = jnp.einsum(
-        "hor,rn->hon",
-        hidden,
-        lax.all_gather(down_weight, "fs", axis=1, tiled=True),
-        preferred_element_type=jnp.float32,
+    partial_value = on_each_block(
+        down_weight,
+        "fs",
+        1,
+        lambda shard, offset: jnp.einsum(
+            "hor,rn->hon", hidden, shard, preferred_element_type=jnp.float32
+        ),
+        2,
     )
     summed = lax.psum_scatter(
         partial_value.astype(jnp.bfloat16), "tp", scatter_dimension=2, tiled=True

time: 486 us -> 440 us (0.905)
  waiting for transfers between devices: 418 us -> 333 us
  starting transfers between devices: 0.28 us -> 36 us
    all_gather x1 -> x0, waiting for transfers between devices: 107 us -> none  [local(): lax.all_gather(down_weight, 'fs', axis=1, tiled=True)]
    ppermute x0 -> x3, waiting for transfers between devices: none -> 100 us  [on_each_block(): lax.ppermute(x, axis, [(d, (d + 1) % ways) for d in range(ways)])]
    all_gather x1, waiting for transfers between devices: 108 us -> 45.2 us  [local(): lax.all_gather(gate_weight, 'fs', axis=0, tiled=True)]
    ppermute x0 -> x3, starting transfers between devices: none -> 35.8 us  [on_each_block(): lax.ppermute(x, axis, [(d, (d + 1) % ways) for d in range(ways)])]
    all_gather x1, waiting for transfers between devices: 17 us -> 0.01 us  [local(): features_full = lax.all_gather(normed_two, 'tp', axis=2, tiled=True)]
    dot_general x1 -> x5, matrix products: 11.3 us -> 13.2 us  [the longest x4 7.33 us: local(): jnp.einsum('hor,rn->hon', hidden, shard, preferred_element_type=jnp.float32)]
  transfers between devices with their start and end apart: 8 -> 10, of which waited for: 8 -> 8; matrix products, arithmetic and copies ran while one was open for 3% -> 5% of each run, Pallas kernels for 0% -> 0%
where the time goes in v1:
time: 440 us
  waiting for transfers between devices  333 us (76%)
  starting transfers between devices  36 us (8%)
  matrix products  24.8 us (6%)
  blocking collectives  23 us (5%)
  between operations  13.8 us (3%)
  other arithmetic  6.85 us (2%)
    all_gather x1, waiting for transfers between devices, local(): lax.all_gather(up_weight, 'fs', axis=0, tiled=True)  101 us
    ppermute x3, waiting for transfers between devices, on_each_block(): lax.ppermute(x, axis, [(d, (d + 1) % ways) for d in range(ways)])  100 us
    all_gather x1, waiting for transfers between devices, local(): lax.all_gather(gate_weight, 'fs', axis=0, tiled=True)  45.2 us
    ppermute x3, starting transfers between devices, on_each_block(): lax.ppermute(x, axis, [(d, (d + 1) % ways) for d in range(ways)])  35.8 us
    reduce_scatter x1, waiting for transfers between devices, local(): lax.psum_scatter(partial_value.astype(jnp.bfloat16), 'tp', scatter_dimens...  26.3 us
    all_gather x1, waiting for transfers between devices, local(): lax.all_gather(normed, 'tp', axis=2, tiled=True)  20.6 us
    all_gather x1, waiting for transfers between devices, local(): in_full = lax.all_gather(in_weight, 'fs', axis=0, tiled=True)  20 us
    all_gather x1, waiting for transfers between devices, local(): out_full = lax.all_gather(out_weight, 'fs', axis=0, tiled=True)  17 us
  transfers between devices with their start and end apart: 10, of which 8 were waited for; matrix products, arithmetic and copies ran while one was open for 5% of the time, Pallas kernels for 0%

profile of v1, /device:TPU:0, one launch (start us, length us, event | category | flops | bytes accessed | tf_op | source)
XLA Modules:
  0.0 439.6 jit_solution(15219113747891514002)
XLA Ops:
  6.5 0.7 all-gather.9.cloned.1.call-update
  7.3 1.2 fusion.16
  8.5 8.4 %psum.14 = f32[1,384]{1,0:T(1,128)S(1)} all-reduce(f32[1,384]{1,0:T(1,128)S(1)} %reduce_sum.23), channel_id=1, replica_groups=mesh['grp'=2,'fs'=4,'tp'=4] {'tp'}, use_global_device_ids=true, to_apply=%region_1.0 | all-reduce | flops 384 | bytes 3072 | tf_op jit(solution)/shard_map/psum | solution.py:41
  16.9 1.9 fusion.18
  18.8 0.7 all-gather.11.cloned.1.call-update
  19.6 20.0 %all-gather.9.cloned.1.call-done = bf16[2048,256]{1,0:T(8,128)(2,1)} async-done(((bf16[512,256]{1,0:T(8,128)(2,1)}), bf16[2048,256]{1,0:T(8,128)(2,1)}) %all-gather.9.cloned.1.call-update) | async-done | bytes 1048592 | tf_op jit(solution)/shard_map/all_gather | solution.py:45
  39.6 20.6 %all-gather.7.cloned.1.call-done = bf16[1,384,2048]{2,1,0:T(8,128)(2,1)} async-done(((bf16[1,384,512]{2,1,0:T(8,128)(2,1)}), bf16[1,384,2048]{2,1,0:T(8,128)(2,1)}) %all-gather.7.cloned.1.call-update) | async-done | bytes 1572880 | tf_op jit(solution)/shard_map/all_gather | solution.py:50
  60.2 2.3 fusion.13
  63.3 0.5 fusion.36
  64.2 8.6 %all_gather.23 = bf16[1,384,1024]{1,2,0:T(8,128)(2,1)S(1)} all-gather(bf16[1,384,256]{1,2,0:T(8,128)(2,1)S(1)} %fusion.35), channel_id=1, replica_groups=mesh['grp'=2,'fs'=4,'tp'=4] {'tp'}, dimensions={2}, use_global_device_ids=true | all-gather | bytes 983040 | tf_op jit(solution)/shard_map/all_gather | solution.py:88
  72.8 17.0 %all-gather.11.cloned.1.call-done = bf16[1024,512]{1,0:T(8,128)(2,1)} async-done(((bf16[256,512]{1,0:T(8,128)(2,1)}), bf16[1024,512]{1,0:T(8,128)(2,1)}) %all-gather.11.cloned.1.call-update) | async-done | bytes 1048592 | tf_op jit(solution)/shard_map/all_gather | solution.py:84
  89.8 1.9 multiply_reduce_fusion
  91.8 6.1 %psum.15 = f32[1,384]{1,0:T(1,128)S(1)} all-reduce(f32[1,384]{1,0:T(1,128)S(1)} %reduce_sum.25), channel_id=1, replica_groups=mesh['grp'=2,'fs'=4,'tp'=4] {'tp'}, use_global_device_ids=true, to_apply=%region_5.6 | all-reduce | flops 384 | bytes 3072 | tf_op jit(solution)/shard_map/psum | solution.py:92
  97.9 0.9 multiply_convert_fusion
  98.8 0.5 all-gather.15.cloned.1.call-update
  99.4 0.5 all-gather.17.cloned.1.call-update
  100.1 1.1 collective-permute-start
  101.3 37.7 %collective-permute-done = bf16[1408,512]{1,0:T(8,128)(2,1)} collective-permute-done((bf16[1408,512]{1,0:T(8,128)(2,1)S(1)}, bf16[1408,512]{1,0:T(8,128)(2,1)}, u32[]{:S(2)}, u32[]{:S(2)}) %collective-permute-start) | collective-permute-done | bytes 1441824 | tf_op jit(solution)/shard_map/ppermute | solution.py:17
  138.9 2.9 collective-permute-start.1
  141.8 62.8 %collective-permute-done.1 = bf16[1408,512]{1,0:T(8,128)(2,1)} collective-permute-done((bf16[1408,512]{1,0:T(8,128)(2,1)}, bf16[1408,512]{1,0:T(8,128)(2,1)}, u32[]{:S(2)}, u32[]{:S(2)}) %collective-permute-start.1) | collective-permute-done | bytes 1441824 | tf_op jit(solution)/shard_map/ppermute | solution.py:17
  204.6 31.7 %collective-permute-start.2 = (bf16[1408,512]{1,0:T(8,128)(2,1)}, bf16[1408,512]{1,0:T(8,128)(2,1)}, u32[]{:S(2)}, u32[]{:S(2)}) collective-permute-start(bf16[1408,512]{1,0:T(8,128)(2,1)} %collective-permute-done.1), channel_id=1, source_target_pairs={{0,4},{4,8},{8,12},{12,0},{1,5},{5,9},{9,13},{13,1},{2,6},{6,10},{... | collective-permute-start | bytes 4325384 | tf_op jit(solution)/shard_map/ppermute | solution.py:17
  236.3 45.2 %all-gather.15.cloned.1.call-done = bf16[2048,1408]{1,0:T(8,128)(2,1)} async-done(((bf16[512,1408]{1,0:T(8,128)(2,1)}), bf16[2048,1408]{1,0:T(8,128)(2,1)}) %all-gather.15.cloned.1.call-update) | async-done | bytes 5767184 | tf_op jit(solution)/shard_map/all_gather | solution.py:100
  281.5 7.2 %fusion.2 = f32[384,1408]{1,0:T(8,128)} fusion(bf16[2048,1408]{1,0:T(8,128)(2,1)} %all-gather.15.cloned.1.call-done, bf16[1,384,2048]{2,1,0:T(8,128)(2,1)} %all-gather.13.cloned.1.call-done), kind=kOutput, calls=%fused_computation.4 | convolution fusion | flops 2214592512 | bytes 9502720 | tf_op jit(solution)/shard_map/slk,kf->slf/dot_general | solution.py:97
  288.7 101.0 %all-gather.17.cloned.1.call-done = bf16[2048,1408]{1,0:T(8,128)(2,1)} async-done(((bf16[512,1408]{1,0:T(8,128)(2,1)}), bf16[2048,1408]{1,0:T(8,128)(2,1)}) %all-gather.17.cloned.1.call-update) | async-done | bytes 5767184 | tf_op jit(solution)/shard_map/all_gather | solution.py:106
  389.7 5.8 %fusion = bf16[384,1408]{1,0:T(8,128)(2,1)S(1)} fusion(bf16[2048,1408]{1,0:T(8,128)(2,1)} %all-gather.17.cloned.1.call-done, f32[384,1408]{1,0:T(8,128)} %fusion.2, bf16[1,384,2048]{2,1,0:T(8,128)(2,1)S(1)} %copy-done.4), kind=kOutput, calls=%fused_computation.2 | convolution fusion | flops 2217836544 | bytes 10584064 | tf_op jit(solution)/shard_map/slk,kf->slf/dot_general | solution.py:103
  395.6 2.1 constant_dynamic-update-slice_fusion.7
  397.7 2.1 constant_dynamic-update-slice_fusion.6
  399.9 2.3 constant_dynamic-update-slice_fusion.5
  402.1 0.8 constant_dynamic-update-slice_fusion.4
  403.1 1.4 dynamic-slice_convert_fusion
  404.5 26.3 %reduce-scatter.2.cloned.1.call-done = bf16[1,384,512]{2,1,0:T(8,128)(2,1)} async-done(((bf16[1,384,2048]{2,1,0:T(8,128)(2,1)}), bf16[1,384,512]{2,1,0:T(8,128)(2,1)}) %reduce-scatter.2.cloned.1.call-update) | async-done | bytes 393232 | tf_op jit(solution)/shard_map/reduce_scatter | solution.py:119
  430.8 1.9 add_convert_fusion
  (55 shorter events, 1.8 us)
Async XLA Ops:
  6.5 57.3 %copy-start = (bf16[2,128,128]{2,1,0:T(8,128)(2,1)S(1)}, bf16[2,128,128]{2,1,0:T(8,128)(2,1)}, u32[]{:S(2)}) copy-start(bf16[2,128,128]{2,1,0:T(8,128)(2,1)} %param.13) | copy-start | bytes 196612
  6.5 33.1 %all-gather.9.cloned.1.call-start = ((), (), s32[]{:S(2)}) async-start(), calls=%async_computation.2 | async-start | bytes 1310720 | tf_op jit(solution)/shard_map/all_gather | solution.py:45
  7.3 53.0 %all-gather.7.cloned.1.call-start = ((), (), s32[]{:S(2)}) async-start(), calls=%async_computation.1 | async-start | bytes 1966080 | tf_op jit(solution)/shard_map/all_gather | solution.py:50
  18.8 71.0 %all-gather.11.cloned.1.call-start = ((), (), s32[]{:S(2)}) async-start(), calls=%async_computation.3 | async-start | bytes 1310720 | tf_op jit(solution)/shard_map/all_gather | solution.py:84
  19.5 216.8 %all-gather.13.cloned.1.call-start = ((), (), s32[]{:S(2)}) async-start(), calls=%async_computation.4 | async-start | bytes 1966080 | tf_op jit(solution)/shard_map/all_gather | solution.py:96
  63.2 0.9 copy-start.3
  63.8 26.1 %copy-start.1 = (bf16[1,384,512]{2,1,0:T(8,128)(2,1)S(1)}, bf16[1,384,512]{2,1,0:T(8,128)(2,1)}, u32[]{:S(2)}) copy-start(bf16[1,384,512]{2,1,0:T(8,128)(2,1)} %param.10) | copy-start | bytes 1179652
  72.8 25.1 %copy-start.2 = (f32[512]{0:T(512)S(1)}, f32[512]{0:T(512)}, u32[]{:S(2)}) copy-start(f32[512]{0:T(512)} %param.16) | copy-start | bytes 6148
  98.8 1.4 copy-start.5
  98.8 182.7 %all-gather.15.cloned.1.call-start = ((), (), s32[]{:S(2)}) async-start(), calls=%async_computation.5 | async-start | bytes 7208960 | tf_op jit(solution)/shard_map/all_gather | solution.py:100
  99.4 290.3 %all-gather.17.cloned.1.call-start = ((), (), s32[]{:S(2)}) async-start(), calls=%async_computation.6 | async-start | bytes 7208960 | tf_op jit(solution)/shard_map/all_gather | solution.py:106
  100.0 330.9 %reduce-scatter.2.cloned.1.call-start = ((), (), s32[]{:S(2)}) async-start(), calls=%async_computation.7 | async-start | bytes 1966080 | tf_op jit(solution)/shard_map/reduce_scatter | solution.py:119
  100.1 38.8 %collective-permute-start = (bf16[1408,512]{1,0:T(8,128)(2,1)S(1)}, bf16[1408,512]{1,0:T(8,128)(2,1)}, u32[]{:S(2)}, u32[]{:S(2)}) collective-permute-start(bf16[1408,512]{1,0:T(8,128)(2,1)S(1)} %copy-done.5), channel_id=1, source_target_pairs={{0,4},{4,8},{8,12},{12,0},{1,5},{5,9},{9,13},{13,1},{2,6},{6,10},{... | collective-permute-start | bytes 4325384 | tf_op jit(solution)/shard_map/ppermute | solution.py:17
  138.9 65.7 %collective-permute-start.1 = (bf16[1408,512]{1,0:T(8,128)(2,1)}, bf16[1408,512]{1,0:T(8,128)(2,1)}, u32[]{:S(2)}, u32[]{:S(2)}) collective-permute-start(bf16[1408,512]{1,0:T(8,128)(2,1)} %collective-permute-done), channel_id=1, source_target_pairs={{0,4},{4,8},{8,12},{12,0},{1,5},{5,9},{9,13},{13,1},{2,6},{6,10},{... | collective-permute-start | bytes 4325384 | tf_op jit(solution)/shard_map/ppermute | solution.py:17
  204.6 190.9 %collective-permute-start.2 = (bf16[1408,512]{1,0:T(8,128)(2,1)}, bf16[1408,512]{1,0:T(8,128)(2,1)}, u32[]{:S(2)}, u32[]{:S(2)}) collective-permute-start(bf16[1408,512]{1,0:T(8,128)(2,1)} %collective-permute-done.1), channel_id=1, source_target_pairs={{0,4},{4,8},{8,12},{12,0},{1,5},{5,9},{9,13},{13,1},{2,6},{6,10},{... | collective-permute-start | bytes 4325384 | tf_op jit(solution)/shard_map/ppermute | solution.py:17
  236.3 153.4 %copy-start.4 = (bf16[1,384,2048]{2,1,0:T(8,128)(2,1)S(1)}, bf16[1,384,2048]{2,1,0:T(8,128)(2,1)}, u32[]{:S(2)}) copy-start(bf16[1,384,2048]{2,1,0:T(8,128)(2,1)} %all-gather.13.cloned.1.call-done) | copy-start | bytes 4718596
  399.9 2.3 copy-start.6
Sparse Core Ops, SparseCore 0:
  8.9 30.6 all-gather.8
  41.2 18.9 all-gather.6
  61.8 27.9 all-gather.10
  98.9 18.8 all-gather.12
  119.2 162.2 all-gather.14
  282.9 106.7 all-gather.16
  404.6 26.1 reduce-scatter.1
